TPU v7x, 32 devices: a whole 2x2x4 slice. The times are simulated.
32 devices in a mesh: grp: 2 (over y), sp: 4 (over z), tp: 4 (over x, core).
Axes of the slice: x: 2, y: 2, z: 4, core: 2. Of those that a mesh axis runs over, the one named last changes fastest.
Arguments:
- queries_small: bfloat16 [2048, 1024], P(('grp', 'sp'), 'tp'), parts along dimension 0, may hold values from -6 to 6
- keys_small: bfloat16 [2048, 512], P(('grp', 'sp'), 'tp'), parts along dimension 0, may hold values from -6 to 6
- values_small: bfloat16 [2048, 512], P(('grp', 'sp'), 'tp'), parts along dimension 0, may hold values from -6 to 6
- queries_large: bfloat16 [2048, 1024], P(('grp', 'sp'), 'tp'), parts along dimension 0, may hold values from -6 to 6
- keys_large: bfloat16 [2048, 512], P(('grp', 'sp'), 'tp'), parts along dimension 0, may hold values from -6 to 6
- values_large: bfloat16 [2048, 512], P(('grp', 'sp'), 'tp'), parts along dimension 0, may hold values from -6 to 6
- query_gain_small: float32 [128], P('grp'), parts along dimension 0, may hold values from 1.2 to 12
- key_gain_small: float32 [128], P('grp'), parts along dimension 0, may hold values from 1.2 to 12
- query_gain_large: float32 [256], P('grp'), parts along dimension 0, may hold values from 1.2 to 12
- key_gain_large: float32 [256], P('grp'), parts along dimension 0, may hold values from 1.2 to 12
- residual_in: bfloat16 [2048, 2048], P(('grp', 'sp', 'tp')), parts along dimension 0, may hold values from -1.5 to 1.5
- out_weight_small: bfloat16 [1024, 2048], P('tp'), may hold values from -0.125 to 0.125
- out_weight_large: bfloat16 [1024, 2048], P('tp'), may hold values from -0.125 to 0.125
- norm_gain: float32 [2048], replicated, may hold values from 0.1 to 1.9
- routes: int32 [2048, 2], P(('grp', 'sp', 'tp')), parts along dimension 0, may hold values from 0 to 7, all different within a row; in each aligned block of 64 rows (0 to 63, 64 to 127, ...) at most 32 rows name the same one
- route_scores: float32 [2048, 2], P(('grp', 'sp', 'tp')), parts along dimension 0, may hold values from 0.05 to 1
- expert_gate: bfloat16 [8, 2048, 1024], P('sp', None, 'tp'), may hold values from -0.125 to 0.125
- expert_up: bfloat16 [8, 2048, 1024], P('sp', None, 'tp'), may hold values from -0.125 to 0.125
- expert_down: bfloat16 [8, 1024, 2048], P('sp', 'tp'), may hold values from -0.1875 to 0.1875
Outputs:
- result: bfloat16 [2048, 2048], P(('grp', 'sp', 'tp')), parts along dimension 0
There are 2 independent parts, one for each index of `grp`. A program takes and returns all parts, laid end to end along the dimension named above; an argument that names none is the same for every part. Nothing has to cross between parts.
Inputs may be any that keep to these rules, and one draw needn't show every extreme that they name: `routes`: each token names 2 different experts; within the rows of one device (aligned blocks of 64 tokens) no expert is named more than 32 times, a bound that some block reaches.
All inputs are finite; a program needn't handle non-finite values.
Results may differ from a plain program's by a relative error of at most 0.02.
The roundings to bfloat16 on the way count: a program that leaves them out, or rounds other values in their place, can miss the bound.
Values may be sent and summed in bfloat16 or wider, within the bound.
A program may use at most 128 MiB of HBM per device.

v0:
```python
import jax
import jax.numpy as jnp
from jax import lax
from jax.sharding import PartitionSpec as P

HS_SMALL = 64
HS_LARGE = 128
GRID_W = 64
theta_base = 10000.0
norm_eps = 1e-06
block_target = 1280


def grid_tables(offset, length, head_size):
    places = offset + jnp.arange(length, dtype=jnp.int32)
    grid_rows = (places // GRID_W).astype(jnp.float32)
    grid_cols = (places % GRID_W).astype(jnp.float32)
    rates = jnp.power(
        theta_base, -2.0 * jnp.arange(head_size // 4, dtype=jnp.float32) / (head_size // 2)
    )
    row_angles = grid_rows[:, None, None] * rates
    col_angles = grid_cols[:, None, None] * rates
    return (jnp.cos(row_angles), jnp.sin(row_angles), jnp.cos(col_angles), jnp.sin(col_angles))


def half_turn(segment, cosine, sine_part):
    half_size = segment.shape[-1] // 2
    leading = segment[..., :half_size]
    trailing = segment[..., half_size:]
    return jnp.concatenate(
        [leading * cosine - trailing * sine_part, trailing * cosine + leading * sine_part], axis=-1
    )


def grid_turn(vectors, tables):
    row_cos, row_sin, col_cos, col_sin = tables
    half_size = vectors.shape[-1] // 2
    return jnp.concatenate(
        [
            half_turn(vectors[..., :half_size], row_cos, row_sin),
            half_turn(vectors[..., half_size:], col_cos, col_sin),
        ],
        axis=-1,
    )


def normed_turn(raw_rows, gain, tables):
    widened = raw_rows.astype(jnp.float32)
    scaled = (
        widened * lax.rsqrt(jnp.mean(widened * widened, axis=-1, keepdims=True) + norm_eps) * gain
    )
    return grid_turn(scaled, tables).astype(jnp.bfloat16)


def block_rows(row_count, shard_rows):
    shards = row_count // shard_rows
    chosen = 1
    for factor in range(1, max(1, block_target // shard_rows) + 1):
        if shards % factor == 0:
            chosen = factor
    return chosen * shard_rows


def attend_block(state, queries, key_rows, value_rows):
    largest, weight_sum, accumulated = state
    head_size = queries.shape[-1]
    kv_local = queries.shape[1]
    key_heads = key_rows.reshape(key_rows.shape[0], kv_local, head_size)
    value_heads = value_rows.reshape(value_rows.shape[0], kv_local, head_size)
    scores = jnp.einsum(
        "qgrd,kgd->qgrk", queries, key_heads, preferred_element_type=jnp.float32
    ) * head_size ** (-0.5)
    peak_score = jnp.maximum(largest, jnp.max(scores, axis=-1))
    shrink = jnp.exp(largest - peak_score)
    weights = jnp.exp(scores - peak_score[..., None])
    weight_sum = weight_sum * shrink + jnp.sum(weights, axis=-1)
    accumulated = accumulated * shrink[..., None] + jnp.einsum(
        "qgrk,kgd->qgrd",
        weights.astype(jnp.bfloat16),
        value_heads,
        preferred_element_type=jnp.float32,
    )
    return (peak_score, weight_sum, accumulated)


def attend_rows(state, queries, key_rows, value_rows):
    row_count = key_rows.shape[0]
    step_rows = block_rows(row_count, queries.shape[0])
    if step_rows == row_count:
        return attend_block(state, queries, key_rows, value_rows)

    def one_block(block_index, carried):
        offset = block_index * step_rows
        return attend_block(
            carried,
            queries,
            lax.dynamic_slice_in_dim(key_rows, offset, step_rows, 0),
            lax.dynamic_slice_in_dim(value_rows, offset, step_rows, 0),
        )

    return lax.fori_loop(0, row_count // step_rows, one_block, state)


def empty_state(queries):
    state_shape = queries.shape[:3]
    return (
        jnp.full(state_shape, -1e30, jnp.float32),
        jnp.zeros(state_shape, jnp.float32),
        jnp.zeros(queries.shape, jnp.float32),
    )


def finish(state):
    largest, weight_sum, accumulated = state
    merged = accumulated / weight_sum[..., None]
    return merged.reshape(merged.shape[0], -1).astype(jnp.bfloat16)


def on_device(
    queries_small,
    keys_small,
    values_small,
    queries_large,
    keys_large,
    values_large,
    query_gain_small,
    key_gain_small,
    query_gain_large,
    key_gain_large,
    residual_in,
    out_weight_small,
    out_weight_large,
    norm_gain,
    routes,
    route_scores,
    expert_gate,
    expert_up,
    expert_down,
):
    token_rows = queries_small.shape[0]
    offset = lax.axis_index("sp") * token_rows
    tables_small = grid_tables(offset, token_rows, HS_SMALL)
    tables_large = grid_tables(offset, token_rows, HS_LARGE)
    kv_small = keys_small.shape[1] // HS_SMALL
    kv_large = keys_large.shape[1] // HS_LARGE
    asked_small = normed_turn(
        queries_small.reshape(token_rows, -1, HS_SMALL), query_gain_small, tables_small
    ).reshape(token_rows, kv_small, -1, HS_SMALL)
    asked_large = normed_turn(
        queries_large.reshape(token_rows, -1, HS_LARGE), query_gain_large, tables_large
    ).reshape(token_rows, kv_large, -1, HS_LARGE)
    turned_small = normed_turn(
        keys_small.reshape(token_rows, kv_small, HS_SMALL), key_gain_small, tables_small
    ).reshape(token_rows, -1)
    turned_large = normed_turn(
        keys_large.reshape(token_rows, kv_large, HS_LARGE), key_gain_large, tables_large
    ).reshape(token_rows, -1)
    key_small = lax.all_gather(turned_small, "sp", axis=0, tiled=True)
    value_small = lax.all_gather(values_small, "sp", axis=0, tiled=True)
    key_large = lax.all_gather(turned_large, "sp", axis=0, tiled=True)
    value_large = lax.all_gather(values_large, "sp", axis=0, tiled=True)
    state_small = attend_rows(empty_state(asked_small), asked_small, key_small, value_small)
    state_large = attend_rows(empty_state(asked_large), asked_large, key_large, value_large)
    heard_small = finish(state_small)
    heard_large = finish(state_large)
    projected = lax.psum_scatter(
        (
            jnp.dot(heard_small, out_weight_small, preferred_element_type=jnp.float32)
            + jnp.dot(heard_large, out_weight_large, preferred_element_type=jnp.float32)
        ).astype(jnp.bfloat16),
        "tp",
        scatter_dimension=0,
        tiled=True,
    ).astype(jnp.float32)
    attended = (residual_in.astype(jnp.float32) + projected).astype(jnp.bfloat16)
    widened = attended.astype(jnp.float32)
    normed = (
        widened
        * lax.rsqrt(jnp.mean(widened * widened, axis=-1, keepdims=True) + norm_eps)
        * norm_gain
    ).astype(jnp.bfloat16)
    local_rows = routes.shape[0]
    top_count = routes.shape[1]
    sp_count = lax.axis_size("sp")
    local_experts = expert_gate.shape[0]
    expert_count = local_experts * sp_count
    capacity = max(2, (2 * top_count * local_rows + expert_count - 1) // expert_count)
    flat_routes = routes.reshape(-1)
    member = (flat_routes[:, None] == jnp.arange(expert_count, dtype=jnp.int32)[None, :]).astype(
        jnp.int32
    )
    ranks = jnp.sum((jnp.cumsum(member, axis=0) - member) * member, axis=1)
    slots = flat_routes * capacity + ranks
    picker = (
        slots[:, None] == jnp.arange(expert_count * capacity, dtype=jnp.int32)[None, :]
    ).astype(jnp.bfloat16)
    placer = jnp.sum(picker.reshape(local_rows, top_count, -1), axis=1)
    outgoing = jnp.einsum("ts,td->sd", placer, normed, preferred_element_type=jnp.float32).astype(
        jnp.bfloat16
    )
    outgoing = outgoing.reshape(sp_count, local_experts, capacity, -1)
    everyone = lax.all_gather(
        lax.all_to_all(outgoing, "sp", split_axis=0, concat_axis=0, tiled=True),
        "tp",
        axis=0,
        tiled=True,
    )
    gate_out = jnp.einsum(
        "secd,edf->secf", everyone, expert_gate, preferred_element_type=jnp.float32
    )
    up_out = jnp.einsum("secd,edf->secf", everyone, expert_up, preferred_element_type=jnp.float32)
    active = (jax.nn.silu(gate_out) * up_out).astype(jnp.bfloat16)
    summed = lax.psum_scatter(
        jnp.einsum(
            "secf,efd->secd", active, expert_down, preferred_element_type=jnp.float32
        ).astype(jnp.bfloat16),
        "tp",
        scatter_dimension=0,
        tiled=True,
    )
    returned = lax.all_to_all(summed, "sp", split_axis=0, concat_axis=0, tiled=True)
    back_rows = returned.reshape(expert_count * capacity, -1)
    chosen_rows = jnp.dot(picker, back_rows, preferred_element_type=jnp.float32).reshape(
        local_rows, top_count, -1
    )
    shares = route_scores / jnp.sum(route_scores, axis=1, keepdims=True)
    mixed = jnp.sum(chosen_rows * shares[:, :, None], axis=1)
    return (attended.astype(jnp.float32) + mixed).astype(jnp.bfloat16)


def solution(mesh):
    in_specs = (
        P(("grp", "sp"), "tp"),
        P(("grp", "sp"), "tp"),
        P(("grp", "sp"), "tp"),
        P(("grp", "sp"), "tp"),
        P(("grp", "sp"), "tp"),
        P(("grp", "sp"), "tp"),
        P("grp"),
        P("grp"),
        P("grp"),
        P("grp"),
        P(("grp", "sp", "tp"), None),
        P("tp", None),
        P("tp", None),
        P(),
        P(("grp", "sp", "tp"), None),
        P(("grp", "sp", "tp"), None),
        P("sp", None, "tp"),
        P("sp", None, "tp"),
        P("sp", "tp", None),
    )
    out_specs = P(("grp", "sp", "tp"), None)
    return jax.shard_map(
        on_device, mesh=mesh, in_specs=in_specs, out_specs=out_specs, check_vma=False
    )
```

profile of v0, /device:TPU:0, one launch (start us, length us, event | category | flops | bytes accessed | tf_op | source)
XLA Modules:
  0.0 313.0 jit_solution(7394251430156797041)
XLA Ops:
  6.6 1.1 copy.83
  9.8 15.7 %all_gather.17 = bf16[1024,128]{0,1:T(8,128)(2,1)S(1)} all-gather(bf16[256,128]{0,1:T(8,128)(2,1)S(1)} %pad_maximum_fusion.1), channel_id=1, replica_groups=mesh['grp'=2,'sp'=4,'tp'=4] {'sp'}, dimensions={0}, use_global_device_ids=true | all-gather | bytes 327680 | tf_op jit(solution)/shard_map/all_gather | solution.py:160
  27.8 1.3 copy-done.2
  29.5 14.4 %all_gather.18 = bf16[1024,128]{0,1:T(8,128)(2,1)S(1)} all-gather(bf16[256,128]{0,1:T(8,128)(2,1)S(1)} %copy.87), channel_id=1, replica_groups=mesh['grp'=2,'sp'=4,'tp'=4] {'sp'}, dimensions={0}, use_global_device_ids=true | all-gather | bytes 327680 | tf_op jit(solution)/shard_map/all_gather | solution.py:161
  44.5 13.8 %all_gather.15 = bf16[1024,128]{0,1:T(8,128)(2,1)S(1)} all-gather(bf16[256,128]{0,1:T(8,128)(2,1)S(1)} %bitcast.168), channel_id=1, replica_groups=mesh['grp'=2,'sp'=4,'tp'=4] {'sp'}, dimensions={0}, use_global_device_ids=true | all-gather | bytes 327680 | tf_op jit(solution)/shard_map/all_gather | solution.py:158
  60.1 1.2 copy-done.1
  61.3 13.8 %all_gather.16 = bf16[1024,128]{1,0:T(8,128)(2,1)S(1)} all-gather(bf16[256,128]{1,0:T(8,128)(2,1)S(1)} %copy-done.8), channel_id=1, replica_groups=mesh['grp'=2,'sp'=4,'tp'=4] {'sp'}, dimensions={0}, use_global_device_ids=true | all-gather | bytes 327680 | tf_op jit(solution)/shard_map/all_gather | solution.py:159
  75.3 3.1 fusion.38
  78.9 1.1 copy-done.3
  80.5 1.5 fusion.3
  83.1 25.4 %reduce-scatter.5.cloned.1.call-done = bf16[64,2048]{1,0:T(8,128)(2,1)} async-done(((bf16[256,2048]{1,0:T(8,128)(2,1)}), bf16[64,2048]{1,0:T(8,128)(2,1)}) %reduce-scatter.5.cloned.1.call-update) | async-done | bytes 262160 | tf_op jit(solution)/shard_map/reduce_scatter | solution.py:166
  108.5 1.1 fusion.48
  109.7 1.4 convolution_convert_fusion
  111.1 30.0 %all_to_all.10 = bf16[4,2,32,2048]{3,2,1,0:T(8,128)(2,1)S(1)} all-to-all(bf16[4,2,32,2048]{3,2,1,0:T(8,128)(2,1)S(1)} %bitcast.163), channel_id=1, replica_groups=mesh['grp'=2,'sp'=4,'tp'=4] {'sp'}, dimensions={0} | all-to-all | bytes 2097152 | tf_op jit(solution)/shard_map/all_to_all | solution.py:203
  141.1 1.0 copy.91
  142.4 32.5 %all-gather.2.cloned.1.call-done = bf16[16,2,32,2048]{3,2,0,1:T(8,128)(2,1)} async-done(((bf16[4,2,32,2048]{3,2,0,1:T(8,128)(2,1)}), bf16[16,2,32,2048]{3,2,0,1:T(8,128)(2,1)}) %all-gather.2.cloned.1.call-update) | async-done | bytes 4194320 | tf_op jit(solution)/shard_map/all_gather | solution.py:202
  174.9 4.1 %fusion.14 = f32[16,2,32,256]{3,2,0,1:T(8,128)S(1)} fusion(bf16[16,2,32,2048]{3,2,0,1:T(8,128)(2,1)} %all-gather.2.cloned.1.call-done, bf16[2,2048,256]{2,1,0:T(8,128)(2,1)} %param.35), kind=kOutput, calls=%fused_computation.21 | convolution fusion | flops 1073741824 | bytes 7340032 | tf_op jit(solution)/shard_map/secd,edf->secf/dot_general | solution.py:208
  179.0 7.3 %convert_bitcast_fusion = bf16[16,2,32,2048]{3,2,0,1:T(8,128)(2,1)} fusion(bf16[2,256,2048]{2,1,0:T(8,128)(2,1)S(1)} %copy-done, bf16[16,2,32,2048]{3,2,0,1:T(8,128)(2,1)} %all-gather.2.cloned.1.call-done, bf16[2,2048,256]{2,1,0:T(8,128)(2,1)} %param.36, f32[16,2,32,256]{3,2,0,1:T(8,128)S(1)} %fusion.14), kind=kOutput, calls=%fused_computation.3 | convolution fusion | flops 2151153664 | bytes 13631488 | tf_op jit(solution)/shard_map/secf,efd->secd/dot_general | solution.py:214
  188.2 83.8 %all-reduce.3.cloned.1.call-done = bf16[16,2,32,2048]{3,2,0,1:T(8,128)(2,1)} async-done(((bf16[16,2,32,2048]{3,2,0,1:T(8,128)(2,1)}), bf16[16,2,32,2048]{3,2,0,1:T(8,128)(2,1)}) %all-reduce.3.cloned.1.call-update) | async-done | bytes 4194320
  272.0 1.3 constant_dynamic-slice_fusion
  273.3 1.1 copy.92
  274.4 4.6 %all-to-all-start.1 = ((bf16[4,2,32,2048]{3,2,1,0:T(8,128)(2,1)}), bf16[4,2,32,2048]{3,2,1,0:T(8,128)(2,1)S(1)}, u32[]{:S(2)}, u32[]{:S(2)}) async-start(bf16[4,2,32,2048]{3,2,1,0:T(8,128)(2,1)} %copy.92), calls=%async_computation.2 | async-start | bytes 2097152 | tf_op jit(solution)/shard_map/all_to_all | solution.py:221
  279.0 25.4 %all-to-all-done.1 = bf16[4,2,32,2048]{3,2,1,0:T(8,128)(2,1)S(1)} async-done(((bf16[4,2,32,2048]{3,2,1,0:T(8,128)(2,1)}), bf16[4,2,32,2048]{3,2,1,0:T(8,128)(2,1)S(1)}, u32[]{:S(2)}, u32[]{:S(2)}) %all-to-all-start.1) | async-done | bytes 1048608 | tf_op jit(solution)/shard_map/all_to_all | solution.py:221
  304.7 1.7 fusion.51
  (92 shorter events, 11.1 us)
Async XLA Ops:
  6.5 172.5 %copy-start = (bf16[2,256,2048]{2,1,0:T(8,128)(2,1)S(1)}, bf16[2,256,2048]{2,1,0:T(8,128)(2,1)}, u32[]{:S(2)}) copy-start(bf16[2,256,2048]{2,1,0:T(8,128)(2,1)} %param.37) | copy-start | bytes 6291460
  6.5 20.1 %copy-start.14 = (f32[128]{0:T(128)S(1)}, f32[128]{0:T(128)}, u32[]{:S(2)}) copy-start(f32[128]{0:T(128)} %param.27) | copy-start | bytes 1540
  6.5 102.0 %reduce-scatter.5.cloned.1.call-start = ((), (), s32[]{:S(2)}) async-start(), calls=%async_computation.3 | async-start | bytes 1310720 | tf_op jit(solution)/shard_map/reduce_scatter | solution.py:166
  27.1 2.4 copy-start.9
  27.1 17.1 %copy-start.10 = (bf16[256,128]{1,0:T(8,128)(2,1)S(1)}, bf16[256,128]{1,0:T(8,128)(2,1)}, u32[]{:S(2)}) copy-start(bf16[256,128]{1,0:T(8,128)(2,1)} %param.20) | copy-start | bytes 196612
  27.7 1.3 copy-start.2
  27.7 16.6 %copy-start.15 = (f32[64]{0:T(128)S(1)}, f32[64]{0:T(128)}, u32[]{:S(2)}) copy-start(f32[64]{0:T(128)} %param.26) | copy-start | bytes 772
  27.7 30.6 %copy-start.7 = (bf16[256,256]{1,0:T(8,128)(2,1)S(1)}, bf16[256,256]{1,0:T(8,128)(2,1)}, u32[]{:S(2)}) copy-start(bf16[256,256]{1,0:T(8,128)(2,1)} %param.19) | copy-start | bytes 393220
  27.7 30.7 %copy-start.16 = (f32[64]{0:T(128)S(1)}, f32[64]{0:T(128)}, u32[]{:S(2)}) copy-start(f32[64]{0:T(128)} %param.25) | copy-start | bytes 772
  59.4 1.9 copy-start.1
  59.4 1.9 copy-start.8
  75.3 3.1 copy-start.5
  78.4 1.6 copy-start.3
  78.9 1.6 copy-start.6
  80.5 1.6 copy-start.12
  80.5 28.0 %copy-start.4 = (bf16[64,2048]{1,0:T(8,128)(2,1)S(1)}, bf16[64,2048]{1,0:T(8,128)(2,1)}, u32[]{:S(2)}) copy-start(bf16[64,2048]{1,0:T(8,128)(2,1)} %param.29) | copy-start | bytes 786436
  80.5 29.1 %copy-start.11 = (f32[2048]{0:T(1024)S(1)}, f32[2048]{0:T(1024)}, u32[]{:S(2)}) copy-start(f32[2048]{0:T(1024)} %param.32) | copy-start | bytes 24580
  82.0 92.9 %all-gather.2.cloned.1.call-start = ((), (), s32[]{:S(2)}) async-start(), calls=%async_computation.4 | async-start | bytes 5242880 | tf_op jit(solution)/shard_map/all_gather | solution.py:202
  142.1 129.9 %all-reduce.3.cloned.1.call-start = ((), (), s32[]{:S(2)}) async-start(), calls=%async_computation.5 | async-start | bytes 8388608
  186.3 0.7 copy-start.17
  273.3 5.7 %copy-start.13 = (f32[64,2]{0,1:T(2,128)S(1)}, f32[64,2]{0,1:T(2,128)}, u32[]{:S(2)}) copy-start(f32[64,2]{0,1:T(2,128)} %param.34) | copy-start | bytes 1540
  274.4 30.0 %all-to-all-start.1 = ((bf16[4,2,32,2048]{3,2,1,0:T(8,128)(2,1)}), bf16[4,2,32,2048]{3,2,1,0:T(8,128)(2,1)S(1)}, u32[]{:S(2)}, u32[]{:S(2)}) async-start(bf16[4,2,32,2048]{3,2,1,0:T(8,128)(2,1)} %copy.92), calls=%async_computation.2 | async-start | bytes 2097152 | tf_op jit(solution)/shard_map/all_to_all | solution.py:221
Sparse Core Ops, SparseCore 0:
  82.1 26.3 reduce-scatter.4
  142.3 32.5 all-gather.1
  186.5 85.4 all-reduce.2
where the time goes:
time: 313 us
  waiting for transfers between devices  167 us (53%)
  blocking collectives  87.7 us (28%)
  matrix products  20.1 us (6%)
  between operations  14.3 us (5%)
  local copies, waits for them, and re-layouts  11.3 us (4%)
  other arithmetic  7.66 us (2%)
  starting transfers between devices  4.86 us (2%)
    unnamed x4, waiting for transfers between devices  83.8 us
    all_gather x1, waiting for transfers between devices, on_device(): lax.all_gather(lax.all_to_all(outgoing, 'sp', split_axis=0, concat_axis=0...  32.5 us
    all_to_all x1, blocking collectives, on_device(): lax.all_to_all(outgoing, 'sp', split_axis=0, concat_axis=0, tiled=True)  30 us
    reduce_scatter x1, waiting for transfers between devices, on_device(): lax.psum_scatter((jnp.dot(heard_small, out_weight_small, preferred_elemen...  25.4 us
    all_to_all x1, waiting for transfers between devices, on_device(): lax.all_to_all(summed, 'sp', split_axis=0, concat_axis=0, tiled=True)  25.4 us
    all_gather x1, blocking collectives, on_device(): key_large = lax.all_gather(turned_large, 'sp', axis=0, tiled=True)  15.7 us
    all_gather x1, blocking collectives, on_device(): value_large = lax.all_gather(values_large, 'sp', axis=0, tiled=True)  14.4 us
    all_gather x1, blocking collectives, on_device(): key_small = lax.all_gather(turned_small, 'sp', axis=0, tiled=True)  13.8 us
  transfers between devices with their start and end apart: 4, of which 4 were waited for; matrix products, arithmetic and copies ran while one was open for 1% of the time, Pallas kernels for 0%

commit v1 on v0

--- a/solution.py
+++ b/solution.py
@@ -2,6 +2,7 @@
 import jax.numpy as jnp
 from jax import lax
 from jax.sharding import PartitionSpec as P
+from jax.lax import axis_index, ppermute, psum
 
 HS_SMALL = 64
 HS_LARGE = 128
@@ -157,7 +158,15 @@
     ).reshape(token_rows, -1)
     key_small = lax.all_gather(turned_small, "sp", axis=0, tiled=True)
     value_small = lax.all_gather(values_small, "sp", axis=0, tiled=True)
-    key_large = lax.all_gather(turned_large, "sp", axis=0, tiled=True)
+    p_count = psum(1, "sp")
+    ledger = [turned_large]
+    for rr in range(p_count - 1):
+        ledger.append(
+            ppermute(ledger[-1], "sp", [(no, (no + 1) % p_count) for no in range(p_count)])
+        )
+    key_large = jnp.roll(
+        jnp.concatenate(ledger[::-1], 0), (axis_index("sp") + 1) * turned_large.shape[0], 0
+    )
     value_large = lax.all_gather(values_large, "sp", axis=0, tiled=True)
     state_small = attend_rows(empty_state(asked_small), asked_small, key_small, value_small)
     state_large = attend_rows(empty_state(asked_large), asked_large, key_large, value_large)

time: 313 us -> 309 us (0.987)
  blocking collectives: 87.7 us -> 71.9 us
  waiting for transfers between devices: 167 us -> 172 us
  starting transfers between devices: 4.86 us -> 8.03 us
    all_gather x1 -> x0, blocking collectives: 15.7 us -> none  [on_device(): key_large = lax.all_gather(turned_large, 'sp', axis=0, tiled=True)]
    ppermute x0 -> x3, waiting for transfers between devices: none -> 5.35 us  [on_device(): ppermute(ledger[-1], 'sp', [(no, (no + 1) % p_count) for no in range(p_co...]
    ppermute x0 -> x3, starting transfers between devices: none -> 3.17 us  [on_device(): ppermute(ledger[-1], 'sp', [(no, (no + 1) % p_count) for no in range(p_co...]
  transfers between devices with their start and end apart: 4 -> 7, of which waited for: 4 -> 5; matrix products, arithmetic and copies ran while one was open for 1% -> 4% of each run, Pallas kernels for 0% -> 0%
where the time goes in v1:
time: 309 us; the launch traced here: 308 us
  waiting for transfers between devices  172 us (56%)
  blocking collectives  71.9 us (23%)
  matrix products  21.4 us (7%)
  between operations  14.3 us (5%)
  local copies, waits for them, and re-layouts  11.1 us (4%)
  other arithmetic  8.95 us (3%)
  starting transfers between devices  8.03 us (3%)
    unnamed x4, waiting for transfers between devices  83.8 us
    all_gather x1, waiting for transfers between devices, on_device(): lax.all_gather(lax.all_to_all(outgoing, 'sp', split_axis=0, concat_axis=0...  32.5 us
    all_to_all x1, blocking collectives, on_device(): lax.all_to_all(outgoing, 'sp', split_axis=0, concat_axis=0, tiled=True)  30 us
    all_to_all x1, waiting for transfers between devices, on_device(): lax.all_to_all(summed, 'sp', split_axis=0, concat_axis=0, tiled=True)  25.4 us
    reduce_scatter x1, waiting for transfers between devices, on_device(): lax.psum_scatter((jnp.dot(heard_small, out_weight_small, preferred_elemen...  25.3 us
    all_gather x1, blocking collectives, on_device(): key_small = lax.all_gather(turned_small, 'sp', axis=0, tiled=True)  14.2 us
    all_gather x1, blocking collectives, on_device(): value_large = lax.all_gather(values_large, 'sp', axis=0, tiled=True)  14 us
    all_gather x1, blocking collectives, on_device(): value_small = lax.all_gather(values_small, 'sp', axis=0, tiled=True)  13.8 us
  transfers between devices with their start and end apart: 7, of which 5 were waited for; matrix products, arithmetic and copies ran while one was open for 4% of the time, Pallas kernels for 0%

profile of v1, /device:TPU:0, one launch (start us, length us, event | category | flops | bytes accessed | tf_op | source)
XLA Modules:
  0.0 308.1 jit_solution(8811530244078643748)
XLA Ops:
  6.6 1.1 copy.83
  9.4 3.1 collective-permute-start
  15.2 14.2 %all_gather.12 = bf16[1024,128]{0,1:T(8,128)(2,1)S(1)} all-gather(bf16[256,128]{0,1:T(8,128)(2,1)S(1)} %bitcast.168), channel_id=1, replica_groups=mesh['grp'=2,'sp'=4,'tp'=4] {'sp'}, dimensions={0}, use_global_device_ids=true | all-gather | bytes 327680 | tf_op jit(solution)/shard_map/all_gather | solution.py:159
  32.7 1.2 copy-done.1
  33.9 13.8 %all_gather.13 = bf16[1024,128]{1,0:T(8,128)(2,1)S(1)} all-gather(bf16[256,128]{1,0:T(8,128)(2,1)S(1)} %copy-done.6), channel_id=1, replica_groups=mesh['grp'=2,'sp'=4,'tp'=4] {'sp'}, dimensions={0}, use_global_device_ids=true | all-gather | bytes 327680 | tf_op jit(solution)/shard_map/all_gather | solution.py:160
  47.9 3.1 %fusion.38 = bf16[256,2,2,64]{0,3,2,1:T(8,128)(2,1)S(1)} fusion(bf16[1024,2,64,1]{0,2,3,1:T(8,128)(2,1)S(1)} %bitcast.166, f32[2,1024,256,2]{2,1,3,0:T(8,128)} %copy-done.1, f32[256,2,2]{0,2,1:T(2,128)S(1)} %broadcast_maximum_fusion, f32[256,2,2]{0,2,1:T(2,128)S(1)} %get-tuple-element.30, f32[256,2,2]{0,2,1:T(2,128)S(1)} %get-tuple-element.29), kind=kOutput, calls=%fused_computation.32 | convolution fusion | flops 137560064 | bytes 4599808 | tf_op jit(solution)/shard_map/qgrk,kgd->qgrd/dot_general | solution.py:78
  51.0 1.8 fusion.119
  53.8 5.3 %collective-permute-done.1 = bf16[256,128]{0,1:T(8,128)(2,1)S(1)} collective-permute-done((bf16[256,128]{0,1:T(8,128)(2,1)S(1)}, bf16[256,128]{0,1:T(8,128)(2,1)S(1)}, u32[]{:S(2)}, u32[]{:S(2)}) %collective-permute-start.1) | collective-permute-done | bytes 65568 | tf_op jit(solution)/shard_map/ppermute | solution.py:165
  59.1 14.0 %all_gather.14 = bf16[1024,128]{0,1:T(8,128)(2,1)S(1)} all-gather(bf16[256,128]{0,1:T(8,128)(2,1)S(1)} %copy.87), channel_id=1, replica_groups=mesh['grp'=2,'sp'=4,'tp'=4] {'sp'}, dimensions={0}, use_global_device_ids=true | all-gather | bytes 327680 | tf_op jit(solution)/shard_map/all_gather | solution.py:170
  75.7 1.5 fusion.3
  78.3 25.3 %reduce-scatter.5.cloned.1.call-done = bf16[64,2048]{1,0:T(8,128)(2,1)} async-done(((bf16[256,2048]{1,0:T(8,128)(2,1)}), bf16[64,2048]{1,0:T(8,128)(2,1)}) %reduce-scatter.5.cloned.1.call-update) | async-done | bytes 262160 | tf_op jit(solution)/shard_map/reduce_scatter | solution.py:175
  103.6 1.1 fusion.48
  104.7 1.4 convolution_convert_fusion
  106.2 30.0 %all_to_all.10 = bf16[4,2,32,2048]{3,2,1,0:T(8,128)(2,1)S(1)} all-to-all(bf16[4,2,32,2048]{3,2,1,0:T(8,128)(2,1)S(1)} %bitcast.163), channel_id=1, replica_groups=mesh['grp'=2,'sp'=4,'tp'=4] {'sp'}, dimensions={0} | all-to-all | bytes 2097152 | tf_op jit(solution)/shard_map/all_to_all | solution.py:212
  136.1 1.0 copy.91
  137.4 32.5 %all-gather.2.cloned.1.call-done = bf16[16,2,32,2048]{3,2,0,1:T(8,128)(2,1)} async-done(((bf16[4,2,32,2048]{3,2,0,1:T(8,128)(2,1)}), bf16[16,2,32,2048]{3,2,0,1:T(8,128)(2,1)}) %all-gather.2.cloned.1.call-update) | async-done | bytes 4194320 | tf_op jit(solution)/shard_map/all_gather | solution.py:211
  170.0 4.1 %fusion.14 = f32[16,2,32,256]{3,2,0,1:T(8,128)S(1)} fusion(bf16[16,2,32,2048]{3,2,0,1:T(8,128)(2,1)} %all-gather.2.cloned.1.call-done, bf16[2,2048,256]{2,1,0:T(8,128)(2,1)} %param.35), kind=kOutput, calls=%fused_computation.21 | convolution fusion | flops 1073741824 | bytes 7340032 | tf_op jit(solution)/shard_map/secd,edf->secf/dot_general | solution.py:217
  174.1 7.3 %convert_bitcast_fusion = bf16[16,2,32,2048]{3,2,0,1:T(8,128)(2,1)} fusion(bf16[2,256,2048]{2,1,0:T(8,128)(2,1)S(1)} %copy-done, bf16[16,2,32,2048]{3,2,0,1:T(8,128)(2,1)} %all-gather.2.cloned.1.call-done, bf16[2,2048,256]{2,1,0:T(8,128)(2,1)} %param.36, f32[16,2,32,256]{3,2,0,1:T(8,128)S(1)} %fusion.14), kind=kOutput, calls=%fused_computation.3 | convolution fusion | flops 2151153664 | bytes 13631488 | tf_op jit(solution)/shard_map/secf,efd->secd/dot_general | solution.py:223
  183.3 83.8 %all-reduce.3.cloned.1.call-done = bf16[16,2,32,2048]{3,2,0,1:T(8,128)(2,1)} async-done(((bf16[16,2,32,2048]{3,2,0,1:T(8,128)(2,1)}), bf16[16,2,32,2048]{3,2,0,1:T(8,128)(2,1)}) %all-reduce.3.cloned.1.call-update) | async-done | bytes 4194320
  267.1 1.3 constant_dynamic-slice_fusion
  268.4 1.1 copy.92
  269.4 4.6 %all-to-all-start.1 = ((bf16[4,2,32,2048]{3,2,1,0:T(8,128)(2,1)}), bf16[4,2,32,2048]{3,2,1,0:T(8,128)(2,1)S(1)}, u32[]{:S(2)}, u32[]{:S(2)}) async-start(bf16[4,2,32,2048]{3,2,1,0:T(8,128)(2,1)} %copy.92), calls=%async_computation.2 | async-start | bytes 2097152 | tf_op jit(solution)/shard_map/all_to_all | solution.py:230
  274.1 25.4 %all-to-all-done.1 = bf16[4,2,32,2048]{3,2,1,0:T(8,128)(2,1)S(1)} async-done(((bf16[4,2,32,2048]{3,2,1,0:T(8,128)(2,1)}), bf16[4,2,32,2048]{3,2,1,0:T(8,128)(2,1)S(1)}, u32[]{:S(2)}, u32[]{:S(2)}) %all-to-all-start.1) | async-done | bytes 1048608 | tf_op jit(solution)/shard_map/all_to_all | solution.py:230
  299.8 1.7 fusion.51
  (99 shorter events, 14.2 us)
Async XLA Ops:
  6.5 167.5 %copy-start = (bf16[2,256,2048]{2,1,0:T(8,128)(2,1)S(1)}, bf16[2,256,2048]{2,1,0:T(8,128)(2,1)}, u32[]{:S(2)}) copy-start(bf16[2,256,2048]{2,1,0:T(8,128)(2,1)} %param.37) | copy-start | bytes 6291460
  6.5 8.3 %copy-start.7 = (bf16[256,128]{1,0:T(8,128)(2,1)S(1)}, bf16[256,128]{1,0:T(8,128)(2,1)}, u32[]{:S(2)}) copy-start(bf16[256,128]{1,0:T(8,128)(2,1)} %param.20) | copy-start | bytes 196612
  6.5 8.5 %copy-start.12 = (f32[64]{0:T(128)S(1)}, f32[64]{0:T(128)}, u32[]{:S(2)}) copy-start(f32[64]{0:T(128)} %param.26) | copy-start | bytes 772
  6.5 97.0 %reduce-scatter.5.cloned.1.call-start = ((), (), s32[]{:S(2)}) async-start(), calls=%async_computation.3 | async-start | bytes 1310720 | tf_op jit(solution)/shard_map/reduce_scatter | solution.py:175
  9.4 43.5 %collective-permute-start = (bf16[256,128]{0,1:T(8,128)(2,1)}, bf16[256,128]{0,1:T(8,128)(2,1)S(1)}, u32[]{:S(2)}, u32[]{:S(2)}) collective-permute-start(bf16[256,128]{0,1:T(8,128)(2,1)} %pad_maximum_fusion.1), channel_id=1, source_target_pairs={{0,4},{4,8},{8,12},{12,0},{1,5},{5,9},{9,13},{13,1},{2,6},{6,10},{... | collective-permute-start | bytes 196616 | tf_op jit(solution)/shard_map/ppermute | solution.py:165
  32.0 1.9 copy-start.1
  32.0 1.9 copy-start.6
  47.9 3.1 %copy-start.4 = (bf16[256,2048]{1,0:T(8,128)(2,1)S(1)}, bf16[256,2048]{1,0:T(8,128)(2,1)}, u32[]{:S(2)}) copy-start(bf16[256,2048]{1,0:T(8,128)(2,1)} %param.30) | copy-start | bytes 3145732
  51.0 1.8 copy-start.13
  52.8 0.8 copy-start.8
  53.0 6.2 %collective-permute-start.1 = (bf16[256,128]{0,1:T(8,128)(2,1)S(1)}, bf16[256,128]{0,1:T(8,128)(2,1)S(1)}, u32[]{:S(2)}, u32[]{:S(2)}) collective-permute-start(bf16[256,128]{0,1:T(8,128)(2,1)S(1)} %collective-permute-done), channel_id=1, source_target_pairs={{0,4},{4,8},{8,12},{12,0},{1,5},{5,9},{9,13},{13,1},{2,6},{6,10},{... | collective-permute-start | bytes 196616 | tf_op jit(solution)/shard_map/ppermute | solution.py:165
  59.1 14.0 %collective-permute-start.2 = (bf16[256,128]{0,1:T(8,128)(2,1)S(1)}, bf16[256,128]{0,1:T(8,128)(2,1)S(1)}, u32[]{:S(2)}, u32[]{:S(2)}) collective-permute-start(bf16[256,128]{0,1:T(8,128)(2,1)S(1)} %collective-permute-done.1), channel_id=1, source_target_pairs={{0,4},{4,8},{8,12},{12,0},{1,5},{5,9},{9,13},{13,1},{2,6},{6,10},{... | collective-permute-start | bytes 196616 | tf_op jit(solution)/shard_map/ppermute | solution.py:165
  73.9 1.6 copy-start.2
  73.9 1.8 copy-start.5
  75.7 1.5 copy-start.10
  75.7 27.9 %copy-start.3 = (bf16[64,2048]{1,0:T(8,128)(2,1)S(1)}, bf16[64,2048]{1,0:T(8,128)(2,1)}, u32[]{:S(2)}) copy-start(bf16[64,2048]{1,0:T(8,128)(2,1)} %param.29) | copy-start | bytes 786436
  75.7 29.0 %copy-start.9 = (f32[2048]{0:T(1024)S(1)}, f32[2048]{0:T(1024)}, u32[]{:S(2)}) copy-start(f32[2048]{0:T(1024)} %param.32) | copy-start | bytes 24580
  77.2 92.8 %all-gather.2.cloned.1.call-start = ((), (), s32[]{:S(2)}) async-start(), calls=%async_computation.4 | async-start | bytes 5242880 | tf_op jit(solution)/shard_map/all_gather | solution.py:211
  137.2 129.9 %all-reduce.3.cloned.1.call-start = ((), (), s32[]{:S(2)}) async-start(), calls=%async_computation.5 | async-start | bytes 8388608
  181.4 0.7 copy-start.14
  268.4 5.7 %copy-start.11 = (f32[64,2]{0,1:T(2,128)S(1)}, f32[64,2]{0,1:T(2,128)}, u32[]{:S(2)}) copy-start(f32[64,2]{0,1:T(2,128)} %param.34) | copy-start | bytes 1540
  269.4 30.0 %all-to-all-start.1 = ((bf16[4,2,32,2048]{3,2,1,0:T(8,128)(2,1)}), bf16[4,2,32,2048]{3,2,1,0:T(8,128)(2,1)S(1)}, u32[]{:S(2)}, u32[]{:S(2)}) async-start(bf16[4,2,32,2048]{3,2,1,0:T(8,128)(2,1)} %copy.92), calls=%async_computation.2 | async-start | bytes 2097152 | tf_op jit(solution)/shard_map/all_to_all | solution.py:230
Sparse Core Ops, SparseCore 0:
  77.3 26.2 reduce-scatter.4
  137.3 32.5 all-gather.1
  181.5 85.4 all-reduce.2
